TPU v7x, 512 devices: a whole 4x8x8 slice. The times are simulated.
512 devices in a mesh: ep: 32 (over z, x), tp: 16 (over y, core).
Axes of the slice: x: 4, y: 8, z: 8, core: 2. Of those that a mesh axis runs over, the one named last changes fastest.
Arguments:
- conv_value: bfloat16 [16384, 2048], P('ep', 'tp'), may hold values from -6 to 6
- conv_gate: bfloat16 [16384, 2048], P('ep', 'tp'), may hold values from -9 to 9
- conv_taps: float32 [31, 2048], P(None, 'tp'), may hold values from -14 to 14
- norm_gain: float32 [2048], P('tp'), may hold values from 0.1 to 1.9
- norm_shift: float32 [2048], P('tp'), may hold values from -3 to 3
- conv_out_weight: bfloat16 [2048, 2048], P(None, 'tp'), may hold values from -0.125 to 0.125
- moe_input: bfloat16 [4096, 2048], P('ep'), may hold values from -6 to 6
- moe_gain: float32 [2048], replicated, may hold values from 0.1 to 1.9
- routes: int32 [4096, 4], P('ep'), may hold values from 0 to 31, all different within a row; in each aligned block of 128 rows (0 to 127, 128 to 255, ...) at most 32 rows name the same one
- route_weights: float32 [4096, 4], P('ep'), may hold values from 0.25 to 1
- expert_gate: bfloat16 [32, 2048, 4096], P('ep', None, 'tp'), may hold values from -0.125 to 0.125
- expert_up: bfloat16 [32, 2048, 4096], P('ep', None, 'tp'), may hold values from -0.125 to 0.125
- expert_down: bfloat16 [32, 4096, 2048], P('ep', None, 'tp'), may hold values from -0.09375 to 0.09375
- shared_gate: bfloat16 [2048, 512], P(None, 'tp'), may hold values from -0.125 to 0.125
- shared_up: bfloat16 [2048, 512], P(None, 'tp'), may hold values from -0.125 to 0.125
- shared_down: bfloat16 [512, 2048], P(None, 'tp'), may hold values from -0.25 to 0.25
Outputs:
- conv_result: bfloat16 [16384, 2048], P('ep', 'tp')
- moe_result: bfloat16 [4096, 2048], P('ep', 'tp')
Inputs may be any that keep to these rules, and one draw needn't show every extreme that they name: `routes`: in the rows of one device (aligned blocks of 128 rows) no expert is named by more than 32 rows, a bound that some block reaches; each row names 4 different experts.
All inputs are finite; a program needn't handle non-finite values.
Results may differ from a plain program's by a relative error of at most 0.0068.
Values may be sent and summed in bfloat16 or wider, within the bound.
A program may use at most 64 MiB of HBM per device.

v0:
```python
import jax
import jax.numpy as jnp
from jax import lax
from jax.sharding import Mesh
from jax.sharding import PartitionSpec as P

EP = ("ep_0", "ep_1")


def from_behind(value, axis, steps):
    count = lax.axis_size(axis)
    initial, last = (max(0, -steps), min(count, count - steps))
    return lax.ppermute(value, axis, [(source, source + steps) for source in range(initial, last)])


def cut_along(array, dim, peers):
    before, after = (array.shape[:dim], array.shape[dim + 1 :])
    return jnp.moveaxis(array.reshape(*before, peers, -1, *after), dim, 0)


def joined_along(parts, dim):
    lengths = list(parts.shape[1:])
    lengths[dim] *= parts.shape[0]
    return jnp.moveaxis(parts, 0, dim).reshape(lengths)


def exchange_in_order(parts, axes, turns):
    lengths = [lax.axis_size(a) for a in axes]
    parts = parts.reshape(*lengths, *parts.shape[1:])
    for k in turns:
        parts = lax.all_to_all(parts, axes[k], split_axis=k, concat_axis=k, tiled=True)
    return parts.reshape(-1, *parts.shape[len(axes) :])


def stepwise_exchange(array, axes, turns, split_dim, concat_dim):
    parts = cut_along(array, split_dim, lax.axis_size(axes))
    return joined_along(exchange_in_order(parts, axes, turns), concat_dim)


def body(
    conv_value,
    conv_gate,
    conv_taps,
    norm_gain,
    norm_shift,
    conv_out_weight,
    moe_input,
    moe_gain,
    routes,
    route_weights,
    expert_gate,
    expert_up,
    expert_down,
    shared_gate,
    shared_up,
    shared_down,
):
    tap_count = conv_taps.shape[0]
    rows_a = conv_value.shape[0]
    glu_rows = (
        conv_value.astype(jnp.float32) * jax.nn.sigmoid(conv_gate.astype(jnp.float32))
    ).astype(jnp.bfloat16)
    before = from_behind(glu_rows[rows_a - (tap_count - 1) :], EP, 1)
    padded = jnp.concatenate([before, glu_rows], axis=0)
    filtered = jnp.zeros(glu_rows.shape, jnp.float32)
    for offset in range(tap_count):
        filtered = filtered + conv_taps[offset] * padded[offset : offset + rows_a].astype(
            jnp.float32
        )
    row_total, squares = lax.psum(
        (jnp.sum(filtered, axis=1), jnp.sum(filtered * filtered, axis=1)), "tp"
    )
    channels = conv_out_weight.shape[0]
    row_mean = row_total / channels
    row_square = squares / channels
    scaled = (filtered - row_mean[:, None]) * lax.rsqrt(row_square - row_mean * row_mean + 1e-05)[
        :, None
    ]
    conv_hidden = jax.nn.silu(scaled * norm_gain + norm_shift).astype(jnp.bfloat16)
    conv_sum = jnp.dot(
        lax.all_gather(conv_hidden, "tp", axis=1, tiled=True),
        conv_out_weight,
        preferred_element_type=jnp.float32,
    )
    conv_result = conv_sum.astype(jnp.bfloat16)
    inputs = moe_input.astype(jnp.float32)
    normed = (
        inputs * lax.rsqrt(jnp.mean(inputs * inputs, axis=1, keepdims=True) + 1e-06) * moe_gain
    ).astype(jnp.bfloat16)
    rows_b, per_row = routes.shape
    model_width = normed.shape[1]
    groups = lax.axis_size(EP)
    capacity = 2 * rows_b * per_row // groups
    flat_expert = routes.reshape(-1)
    owner_row = jnp.arange(rows_b * per_row, dtype=jnp.int32) // per_row
    expert_hits = (flat_expert[:, None] == jnp.arange(groups, dtype=jnp.int32)[None, :]).astype(
        jnp.int32
    )
    slot_rank = jnp.sum((jnp.cumsum(expert_hits, axis=0) - expert_hits) * expert_hits, axis=1)
    slot_index = flat_expert * capacity + slot_rank
    outgoing = (
        jnp.zeros((groups * capacity, model_width), jnp.bfloat16)
        .at[slot_index]
        .set(normed[owner_row])
    )
    outgoing = outgoing.reshape(groups, capacity, model_width)
    slot_share = capacity // lax.axis_size("tp")
    own_slots = lax.dynamic_slice_in_dim(outgoing, lax.axis_index("tp") * slot_share, slot_share, 1)
    partial_rows = lax.all_to_all(own_slots, EP, split_axis=0, concat_axis=0, tiled=True)
    arrived = lax.all_gather(partial_rows, "tp", axis=1, tiled=True)
    arrived_rows = arrived.reshape(groups * capacity, model_width)
    gate_value = jnp.dot(arrived_rows, expert_gate[0], preferred_element_type=jnp.float32)
    upward = jnp.dot(arrived_rows, expert_up[0], preferred_element_type=jnp.float32)
    expert_hidden = (jax.nn.silu(gate_value) * upward).astype(jnp.bfloat16)
    shared_hidden = (
        jax.nn.silu(jnp.dot(normed, shared_gate, preferred_element_type=jnp.float32))
        * jnp.dot(normed, shared_up, preferred_element_type=jnp.float32)
    ).astype(jnp.bfloat16)
    columns = expert_down.shape[2]
    routed_rows = expert_down[0]
    routed_sum = jnp.dot(
        lax.all_gather(expert_hidden, "tp", axis=1, tiled=True),
        routed_rows,
        preferred_element_type=jnp.float32,
    )
    shared_sum = jnp.dot(
        lax.all_gather(shared_hidden, "tp", axis=1, tiled=True),
        shared_down,
        preferred_element_type=jnp.float32,
    )
    expert_out = routed_sum.astype(jnp.bfloat16).reshape(groups, capacity, columns)
    returned = stepwise_exchange(expert_out, EP, (0, 1), 0, 0).reshape(groups * capacity, columns)
    picked = returned[slot_index].astype(jnp.float32) * route_weights.reshape(-1)[:, None]
    moe_sum = jnp.sum(picked.reshape(rows_b, per_row, columns), axis=1) + shared_sum
    return (conv_result, moe_sum.astype(jnp.bfloat16))


def solution(mesh):
    finer = Mesh(mesh.devices.reshape(8, 4, mesh.shape["tp"]), ("ep_0", "ep_1", "tp"))
    in_specs = (
        P(EP, "tp"),
        P(EP, "tp"),
        P(None, "tp"),
        P("tp"),
        P("tp"),
        P(None, "tp"),
        P(EP, None),
        P(),
        P(EP, None),
        P(EP, None),
        P(EP, None, "tp"),
        P(EP, None, "tp"),
        P(EP, None, "tp"),
        P(None, "tp"),
        P(None, "tp"),
        P(None, "tp"),
    )
    out_specs = (P(EP, "tp"), P(EP, "tp"))
    return jax.shard_map(body, mesh=finer, in_specs=in_specs, out_specs=out_specs, check_vma=False)
```

profile of v0, /device:TPU:1, one launch (start us, length us, event | category | flops | bytes accessed | tf_op | source)
XLA Modules:
  0.0 226.3 jit_solution(18367188397835349781)
XLA Ops:
  7.2 0.8 broadcast_multiply_fusion
  8.0 0.8 copy.33
  9.0 1.2 fusion.6
  10.5 1.2 reduce-window.6
  11.7 0.2 slice_reduce_fusion
  12.1 1.2 fusion.8
  13.3 12.8 %scatter_custom_fusion = bf16[1024,2048]{1,0:T(8,128)(2,1)} fusion(s32[512]{0:T(512)S(1)} %bitcast.118, bf16[128,2048]{1,0:T(8,128)(2,1)S(1)} %fusion.8, s32[1024]{0:T(1024)S(1)} %pad_clamp_fusion.1, bf16[]{:T(256)} %constant.47.clone.1), kind=kCustom, calls=%fused_computation.3 | custom fusion | bytes 4194306 | tf_op jit(solution)/shard_map/scatter | solution.py:104
  26.1 1.5 constant_dynamic-slice_fusion
  27.6 24.8 %all_to_all.15 = bf16[32,2,2048]{2,1,0:T(2,128)(2,1)S(1)} all-to-all(bf16[32,2,2048]{2,1,0:T(2,128)(2,1)S(1)} %constant_dynamic-slice_fusion), channel_id=1, replica_groups=mesh['ep_0'=8,'ep_1'=4,'tp'=16] {'ep_0','ep_1'}, dimensions={0} | all-to-all | bytes 524288 | tf_op jit(solution)/shard_map/all_to_all | solution.py:109
  52.4 0.8 copy.36
  53.3 42.1 %all-gather.6.cloned.1.call-done = bf16[32,32,2048]{2,0,1:T(8,128)(2,1)} async-done(((bf16[32,2,2048]{2,0,1:T(8,128)(2,1)}), bf16[32,32,2048]{2,0,1:T(8,128)(2,1)}) %all-gather.6.cloned.1.call-update) | async-done | bytes 4194320 | tf_op jit(solution)/shard_map/all_gather | solution.py:110
  95.4 4.5 %copy.37 = bf16[32,32,2048]{2,1,0:T(8,128)(2,1)S(1)} copy(bf16[32,32,2048]{2,0,1:T(8,128)(2,1)} %all-gather.6.cloned.1.call-done) | data formatting | bytes 8388608 | tf_op jit(solution)/shard_map/all_gather | solution.py:110
  99.9 1.3 fusion.11
  101.2 2.1 fusion.3
  103.5 3.1 %collective-permute-start = (bf16[30,128]{1,0:T(8,128)(2,1)S(1)}, bf16[30,128]{1,0:T(8,128)(2,1)S(1)}, u32[]{:S(2)}, u32[]{:S(2)}) collective-permute-start(bf16[30,128]{1,0:T(8,128)(2,1)S(1)} %slice.260), channel_id=1, source_target_pairs={{0,16},{16,32},{32,48},{48,64},{64,80},{80,96},{96,112},{112,128},... | collective-permute-start | bytes 23048 | tf_op jit(solution)/shard_map/ppermute | solution.py:13
  106.7 0.7 collective-permute-done
  107.4 1.2 fusion.47
  108.6 25.0 %all-reduce = (f32[512]{0:T(512)S(1)}, f32[512]{0:T(512)S(1)}) all-reduce(f32[512]{0:T(512)S(1)} %get-tuple-element.3, f32[512]{0:T(512)S(1)} %get-tuple-element.2), channel_id=1, replica_groups=mesh['ep_0'=8,'ep_1'=4,'tp'=16] {'tp'}, use_global_device_ids=true, to_apply=%region_3.0 | all-reduce | flops 1024 | bytes 8192 | tf_op jit(solution)/shard_map/psum | solution.py:70
  133.7 0.9 multiply_convert_fusion
  134.6 35.8 %all-gather.8.cloned.1.call-done = bf16[1024,4096]{1,0:T(8,128)(2,1)} async-done(((bf16[1024,256]{1,0:T(8,128)(2,1)}), bf16[1024,4096]{1,0:T(8,128)(2,1)}) %all-gather.8.cloned.1.call-update) | async-done | bytes 8388624 | tf_op jit(solution)/shard_map/all_gather | solution.py:122
  170.4 6.7 %convolution_convert_fusion = bf16[1024,128]{1,0:T(8,128)(2,1)} fusion(bf16[1024,4096]{1,0:T(8,128)(2,1)} %all-gather.8.cloned.1.call-done, bf16[1,4096,128]{2,1,0:T(8,128)(2,1)} %param.28), kind=kOutput, calls=%fused_computation.39 | convolution fusion | flops 1073872896 | bytes 9699328 | tf_op jit(solution)/shard_map/dot_general | solution.py:121
  177.1 6.5 %all-to-all-start.1 = ((bf16[8,4,1,32,128]{4,3,1,2,0:T(8,128)(2,1)}), bf16[8,4,1,32,128]{4,3,1,2,0:T(8,128)(2,1)S(1)}, u32[]{:S(2)}, u32[]{:S(2)}) async-start(bf16[8,4,1,32,128]{4,3,1,2,0:T(8,128)(2,1)} %bitcast.41), calls=%async_computation.1 | async-start | bytes 524288 | tf_op jit(solution)/shard_map/all_to_all | solution.py:31
  183.6 0.3 fusion.48
  184.1 0.3 fusion.5
  184.3 16.1 %all_gather.15 = bf16[128,512]{0,1:T(8,128)(2,1)S(1)} all-gather(bf16[128,32]{0,1:T(8,128)(2,1)S(1)} %fusion.5), channel_id=1, replica_groups=mesh['ep_0'=8,'ep_1'=4,'tp'=16] {'tp'}, dimensions={1}, use_global_device_ids=true | all-gather | bytes 139264 | tf_op jit(solution)/shard_map/all_gather | solution.py:127
  200.4 0.7 copy.39
  201.1 4.1 %all-to-all-start.2 = ((bf16[8,4,1,32,128]{4,3,0,2,1:T(8,128)(2,1)}), bf16[8,4,1,32,128]{4,3,0,2,1:T(8,128)(2,1)S(1)}, u32[]{:S(2)}, u32[]{:S(2)}) async-start(bf16[8,4,1,32,128]{4,3,0,2,1:T(8,128)(2,1)} %copy.39), calls=%async_computation.2 | async-start | bytes 524288 | tf_op jit(solution)/shard_map/all_to_all | solution.py:31
  205.2 9.1 %all-gather.4.cloned.1.call-done = bf16[512,2048]{1,0:T(8,128)(2,1)} async-done(((bf16[512,128]{1,0:T(8,128)(2,1)}), bf16[512,2048]{1,0:T(8,128)(2,1)}) %all-gather.4.cloned.1.call-update) | async-done | bytes 2097168 | tf_op jit(solution)/shard_map/all_gather | solution.py:81
  214.3 3.0 %convolution_convert_fusion.1 = bf16[512,128]{1,0:T(8,128)(2,1)} fusion(bf16[512,2048]{1,0:T(8,128)(2,1)} %all-gather.4.cloned.1.call-done, bf16[2048,128]{1,0:T(8,128)(2,1)S(1)} %copy-done.1), kind=kOutput, calls=%fused_computation.40 | convolution fusion | flops 268500992 | bytes 2752512 | tf_op jit(solution)/shard_map/dot_general | solution.py:80
  217.3 1.3 gather_fusion
  218.6 0.2 fusion.13
  218.9 0.8 fusion.4
  (52 shorter events, 1.1 us)
Async XLA Ops:
  7.2 92.7 %copy-start = (bf16[1,2048,256]{2,1,0:T(8,128)(2,1)S(1)}, bf16[1,2048,256]{2,1,0:T(8,128)(2,1)}, u32[]{:S(2)}) copy-start(bf16[1,2048,256]{2,1,0:T(8,128)(2,1)} %param.26) | copy-start | bytes 3145732
  7.2 88.2 %all-gather.6.cloned.1.call-start = ((), (), s32[]{:S(2)}) async-start(), calls=%async_computation.4 | async-start | bytes 4456448 | tf_op jit(solution)/shard_map/all_gather | solution.py:110
  53.2 117.2 %all-gather.8.cloned.1.call-start = ((), (), s32[]{:S(2)}) async-start(), calls=%async_computation.5 | async-start | bytes 8912896 | tf_op jit(solution)/shard_map/all_gather | solution.py:122
  99.9 1.3 copy-start.11
  101.2 2.3 copy-start.2
  101.2 2.3 copy-start.3
  101.2 5.5 %copy-start.7 = (f32[31,128]{1,0:T(8,128)S(1)}, f32[31,128]{1,0:T(8,128)}, u32[]{:S(2)}) copy-start(f32[31,128]{1,0:T(8,128)} %param.18) | copy-start | bytes 47620
  101.2 32.4 %copy-start.9 = (f32[128]{0:T(128)S(1)}, f32[128]{0:T(128)}, u32[]{:S(2)}) copy-start(f32[128]{0:T(128)} %param.20) | copy-start | bytes 1540
  101.2 32.4 %copy-start.10 = (f32[128]{0:T(128)S(1)}, f32[128]{0:T(128)}, u32[]{:S(2)}) copy-start(f32[128]{0:T(128)} %param.19) | copy-start | bytes 1540
  103.4 110.9 %all-gather.4.cloned.1.call-start = ((), (), s32[]{:S(2)}) async-start(), calls=%async_computation.3 | async-start | bytes 2228224 | tf_op jit(solution)/shard_map/all_gather | solution.py:81
  103.5 3.9 %collective-permute-start = (bf16[30,128]{1,0:T(8,128)(2,1)S(1)}, bf16[30,128]{1,0:T(8,128)(2,1)S(1)}, u32[]{:S(2)}, u32[]{:S(2)}) collective-permute-start(bf16[30,128]{1,0:T(8,128)(2,1)S(1)} %slice.260), channel_id=1, source_target_pairs={{0,16},{16,32},{32,48},{48,64},{64,80},{80,96},{96,112},{112,128},... | collective-permute-start | bytes 23048 | tf_op jit(solution)/shard_map/ppermute | solution.py:13
  134.6 49.1 %copy-start.4 = (bf16[2048,32]{0,1:T(8,128)(2,1)S(1)}, bf16[2048,32]{0,1:T(8,128)(2,1)}, u32[]{:S(2)}) copy-start(bf16[2048,32]{0,1:T(8,128)(2,1)} %param.29) | copy-start | bytes 393220
  134.6 49.3 %copy-start.8 = (f32[128,4]{0,1:T(4,128)S(1)}, f32[128,4]{0,1:T(4,128)}, u32[]{:S(2)}) copy-start(f32[128,4]{0,1:T(4,128)} %param.25) | copy-start | bytes 6148
  134.6 49.5 %copy-start.5 = (bf16[2048,32]{0,1:T(8,128)(2,1)S(1)}, bf16[2048,32]{0,1:T(8,128)(2,1)}, u32[]{:S(2)}) copy-start(bf16[2048,32]{0,1:T(8,128)(2,1)} %param.30) | copy-start | bytes 393220
  134.6 79.7 %copy-start.1 = (bf16[2048,128]{1,0:T(8,128)(2,1)S(1)}, bf16[2048,128]{1,0:T(8,128)(2,1)}, u32[]{:S(2)}) copy-start(bf16[2048,128]{1,0:T(8,128)(2,1)} %param.21) | copy-start | bytes 1572868
  177.1 41.8 %copy-start.6 = (bf16[512,128]{1,0:T(8,128)(2,1)S(1)}, bf16[512,128]{1,0:T(8,128)(2,1)}, u32[]{:S(2)}) copy-start(bf16[512,128]{1,0:T(8,128)(2,1)} %param.31) | copy-start | bytes 393220
  177.1 23.3 %all-to-all-start.1 = ((bf16[8,4,1,32,128]{4,3,1,2,0:T(8,128)(2,1)}), bf16[8,4,1,32,128]{4,3,1,2,0:T(8,128)(2,1)S(1)}, u32[]{:S(2)}, u32[]{:S(2)}) async-start(bf16[8,4,1,32,128]{4,3,1,2,0:T(8,128)(2,1)} %bitcast.41), calls=%async_computation.1 | async-start | bytes 524288 | tf_op jit(solution)/shard_map/all_to_all | solution.py:31
  201.1 16.1 %all-to-all-start.2 = ((bf16[8,4,1,32,128]{4,3,0,2,1:T(8,128)(2,1)}), bf16[8,4,1,32,128]{4,3,0,2,1:T(8,128)(2,1)S(1)}, u32[]{:S(2)}, u32[]{:S(2)}) async-start(bf16[8,4,1,32,128]{4,3,0,2,1:T(8,128)(2,1)} %copy.39), calls=%async_computation.2 | async-start | bytes 524288 | tf_op jit(solution)/shard_map/all_to_all | solution.py:31
Sparse Core Ops, SparseCore 0:
  53.3 42.0 all-gather.5
  103.5 66.8 all-gather.7
  173.1 41.1 all-gather.3
where the time goes:
time: 227 us; the launch traced here: 226 us
  waiting for transfers between devices  87.8 us (39%)
  blocking collectives  65.9 us (29%)
  local copies, waits for them, and re-layouts  23.3 us (10%)
  matrix products  14.4 us (6%)
  between operations  14 us (6%)
  starting transfers between devices  13.8 us (6%)
  other arithmetic  6.99 us (3%)
    all_gather x1, waiting for transfers between devices, body(): arrived = lax.all_gather(partial_rows, 'tp', axis=1, tiled=True)  42.1 us
    all_gather x1, waiting for transfers between devices, body(): lax.all_gather(expert_hidden, 'tp', axis=1, tiled=True)  35.8 us
    psum x1, blocking collectives, body(): lax.psum((jnp.sum(filtered, axis=1), jnp.sum(filtered * filtered, axis=1)...  25 us
    all_to_all x1, blocking collectives, body(): lax.all_to_all(own_slots, EP, split_axis=0, concat_axis=0, tiled=True)  24.8 us
    all_gather x1, blocking collectives, body(): lax.all_gather(shared_hidden, 'tp', axis=1, tiled=True)  16.1 us
    scatter x1, local copies, waits for them, and re-layouts, body(): outgoing = jnp.zeros((groups * capacity, model_width), jnp.bfloat16).at[s...  12.8 us
    all_to_all x2, starting transfers between devices, exchange_in_order(): lax.all_to_all(parts, axes[k], split_axis=k, concat_axis=k, tiled=True)  10.6 us
    all_gather x1, waiting for transfers between devices, body(): lax.all_gather(conv_hidden, 'tp', axis=1, tiled=True)  9.08 us
  transfers between devices with their start and end apart: 6, of which 4 were waited for; matrix products, arithmetic and copies ran while one was open for 6% of the time, Pallas kernels for 0%

commit v1 on v0

--- a/solution.py
+++ b/solution.py
@@ -119,7 +119,9 @@
     columns = expert_down.shape[2]
     routed_rows = expert_down[0]
     routed_sum = jnp.dot(
-        lax.all_gather(expert_hidden, "tp", axis=1, tiled=True),
+        jnp.concatenate(
+            lax.all_to_all(jnp.stack([expert_hidden] * lax.axis_size("tp")), "tp", 0, 0), axis=1
+        ),
         routed_rows,
         preferred_element_type=jnp.float32,
     )

time: 227 us -> 373 us (1.64)
  blocking collectives: 65.9 us -> 237 us
  waiting for transfers between devices: 87.8 us -> 52.7 us
  starting transfers between devices: 13.8 us -> 19.2 us
  local copies, waits for them, and re-layouts: 23.3 us -> 27.8 us
    psum x1, blocking collectives: 25 us -> 196 us  [body(): lax.psum((jnp.sum(filtered, axis=1), jnp.sum(filtered * filtered, axis=1)...]
    all_gather x1 -> x0, waiting for transfers between devices: 35.8 us -> none  [body(): lax.all_gather(expert_hidden, 'tp', axis=1, tiled=True)]
    all_to_all x0 -> x1, starting transfers between devices: none -> 4.88 us  [body(): lax.all_to_all(jnp.stack([expert_hidden] * lax.axis_size('tp')), 'tp', 0, 0)]
    another operation x1 -> x2, local copies, waits for them, and re-layouts: 0.01 us -> 4.3 us  [the longest x1 4.29 us: body(): jnp.stack([expert_hidden] * lax.axis_size('tp'))]
  transfers between devices with their start and end apart: 6 -> 6, of which waited for: 4 -> 3; matrix products, arithmetic and copies ran while one was open for 6% -> 4% of each run, Pallas kernels for 0% -> 0%
where the time goes in v1:
time: 373 us; the launch traced here: 372 us
  blocking collectives  237 us (64%)
  waiting for transfers between devices  52.7 us (14%)
  local copies, waits for them, and re-layouts  27.8 us (7%)
  starting transfers between devices  19.2 us (5%)
  between operations  14.3 us (4%)
  matrix products  13.7 us (4%)
  other arithmetic  6.99 us (2%)
    psum x1, blocking collectives, body(): lax.psum((jnp.sum(filtered, axis=1), jnp.sum(filtered * filtered, axis=1)...  196 us
    all_gather x1, waiting for transfers between devices, body(): arrived = lax.all_gather(partial_rows, 'tp', axis=1, tiled=True)  42.2 us
    all_to_all x1, blocking collectives, body(): lax.all_to_all(own_slots, EP, split_axis=0, concat_axis=0, tiled=True)  24.8 us
    all_gather x1, blocking collectives, body(): lax.all_gather(shared_hidden, 'tp', axis=1, tiled=True)  16.5 us
    scatter x1, local copies, waits for them, and re-layouts, body(): outgoing = jnp.zeros((groups * capacity, model_width), jnp.bfloat16).at[s...  12.8 us
    all_to_all x2, starting transfers between devices, exchange_in_order(): lax.all_to_all(parts, axes[k], split_axis=k, concat_axis=k, tiled=True)  11.2 us
    all_gather x1, waiting for transfers between devices, body(): lax.all_gather(conv_hidden, 'tp', axis=1, tiled=True)  9.75 us
  transfers between devices with their start and end apart: 6, of which 3 were waited for; matrix products, arithmetic and copies ran while one was open for 4% of the time, Pallas kernels for 0%

profile of v1, /device:TPU:1, one launch (start us, length us, event | category | flops | bytes accessed | tf_op | source)
XLA Modules:
  0.0 372.0 jit_solution(7749784929222617143)
XLA Ops:
  7.2 0.8 broadcast_multiply_fusion
  8.0 0.8 copy.35
  9.0 1.2 fusion.6
  10.5 1.2 reduce-window.6
  12.1 1.2 fusion.8
  13.3 12.8 %scatter_custom_fusion = bf16[1024,2048]{1,0:T(8,128)(2,1)} fusion(s32[512]{0:T(512)S(1)} %bitcast.121, bf16[128,2048]{1,0:T(8,128)(2,1)S(1)} %fusion.8, s32[1024]{0:T(1024)S(1)} %pad_clamp_fusion.1, bf16[]{:T(256)} %constant.47.clone.1), kind=kCustom, calls=%fused_computation.3 | custom fusion | bytes 4194306 | tf_op jit(solution)/shard_map/scatter | solution.py:104
  26.1 1.5 constant_dynamic-slice_fusion
  27.6 24.8 %all_to_all.20 = bf16[32,2,2048]{2,1,0:T(2,128)(2,1)S(1)} all-to-all(bf16[32,2,2048]{2,1,0:T(2,128)(2,1)S(1)} %constant_dynamic-slice_fusion), channel_id=1, replica_groups=mesh['ep_0'=8,'ep_1'=4,'tp'=16] {'ep_0','ep_1'}, dimensions={0} | all-to-all | bytes 524288 | tf_op jit(solution)/shard_map/all_to_all | solution.py:109
  52.4 0.8 copy.38
  53.2 42.2 %all-gather.5.cloned.1.call-done = bf16[32,32,2048]{2,0,1:T(8,128)(2,1)} async-done(((bf16[32,2,2048]{2,0,1:T(8,128)(2,1)}), bf16[32,32,2048]{2,0,1:T(8,128)(2,1)}) %all-gather.5.cloned.1.call-update) | async-done | bytes 4194320 | tf_op jit(solution)/shard_map/all_gather | solution.py:110
  95.4 4.5 %copy.39 = bf16[32,32,2048]{2,1,0:T(8,128)(2,1)S(1)} copy(bf16[32,32,2048]{2,0,1:T(8,128)(2,1)} %all-gather.5.cloned.1.call-done) | data formatting | bytes 8388608 | tf_op jit(solution)/shard_map/all_gather | solution.py:110
  99.9 1.3 fusion.11
  101.2 1.3 fusion.3
  102.7 4.3 %stack.2 = bf16[16,1024,256]{1,2,0:T(8,128)(2,1)} broadcast(bf16[1024,256]{0,1:T(8,128)(2,1)S(1)} %copy.40), dimensions={1,2} | broadcast | bytes 8912896 | tf_op jit(solution)/shard_map/stack | solution.py:123
  107.0 4.9 %all-to-all-start.1 = ((bf16[16,1024,256]{1,2,0:T(8,128)(2,1)}), bf16[16,1024,256]{1,2,0:T(8,128)(2,1)}, u32[]{:S(2)}, u32[]{:S(2)}) async-start(bf16[16,1024,256]{1,2,0:T(8,128)(2,1)} %stack.2), calls=%async_computation.1 | async-start | bytes 16777216 | tf_op jit(solution)/shard_map/all_to_all | solution.py:123
  112.1 3.1 collective-permute-start
  115.2 0.7 collective-permute-done
  115.9 1.2 fusion.47
  117.1 195.9 %all-reduce = (f32[512]{0:T(512)S(1)}, f32[512]{0:T(512)S(1)}) all-reduce(f32[512]{0:T(512)S(1)} %get-tuple-element.3, f32[512]{0:T(512)S(1)} %get-tuple-element.2), channel_id=1, replica_groups=mesh['ep_0'=8,'ep_1'=4,'tp'=16] {'tp'}, use_global_device_ids=true, to_apply=%region_3.0 | all-reduce | flops 1024 | bytes 8192 | tf_op jit(solution)/shard_map/psum | solution.py:70
  313.1 0.9 multiply_convert_fusion
  314.1 6.8 %convolution_convert_fusion = bf16[1024,128]{1,0:T(8,128)(2,1)} fusion(bf16[1024,4096]{0,1:T(8,128)(2,1)} %bitcast.40, bf16[1,4096,128]{2,1,0:T(8,128)(2,1)} %param.28), kind=kOutput, calls=%fused_computation.39 | convolution fusion | flops 1073872896 | bytes 9699328 | tf_op jit(solution)/shard_map/dot_general | solution.py:121
  320.9 7.2 %all-to-all-start.2 = ((bf16[8,4,1,32,128]{4,3,1,2,0:T(8,128)(2,1)}), bf16[8,4,1,32,128]{4,3,1,2,0:T(8,128)(2,1)S(1)}, u32[]{:S(2)}, u32[]{:S(2)}) async-start(bf16[8,4,1,32,128]{4,3,1,2,0:T(8,128)(2,1)} %bitcast.43), calls=%async_computation.2 | async-start | bytes 524288 | tf_op jit(solution)/shard_map/all_to_all | solution.py:31
  328.1 0.3 fusion.48
  328.5 0.3 fusion.5
  328.8 16.5 %all_gather.11 = bf16[128,512]{0,1:T(8,128)(2,1)S(1)} all-gather(bf16[128,32]{0,1:T(8,128)(2,1)S(1)} %fusion.5), channel_id=1, replica_groups=mesh['ep_0'=8,'ep_1'=4,'tp'=16] {'tp'}, dimensions={1}, use_global_device_ids=true | all-gather | bytes 139264 | tf_op jit(solution)/shard_map/all_gather | solution.py:129
  345.3 0.7 copy.42
  346.0 4.0 %all-to-all-start.3 = ((bf16[8,4,1,32,128]{4,3,0,2,1:T(8,128)(2,1)}), bf16[8,4,1,32,128]{4,3,0,2,1:T(8,128)(2,1)S(1)}, u32[]{:S(2)}, u32[]{:S(2)}) async-start(bf16[8,4,1,32,128]{4,3,0,2,1:T(8,128)(2,1)} %copy.42), calls=%async_computation.3 | async-start | bytes 524288 | tf_op jit(solution)/shard_map/all_to_all | solution.py:31
  350.0 9.8 %all-gather.3.cloned.1.call-done = bf16[512,2048]{1,0:T(8,128)(2,1)} async-done(((bf16[512,128]{1,0:T(8,128)(2,1)}), bf16[512,2048]{1,0:T(8,128)(2,1)}) %all-gather.3.cloned.1.call-update) | async-done | bytes 2097168 | tf_op jit(solution)/shard_map/all_gather | solution.py:81
  359.7 3.0 convolution_convert_fusion.1
  362.7 1.3 gather_fusion
  364.1 0.2 fusion.13
  364.3 0.8 fusion.4
  (53 shorter events, 1.5 us)
Async XLA Ops:
  7.2 92.7 %copy-start = (bf16[1,2048,256]{2,1,0:T(8,128)(2,1)S(1)}, bf16[1,2048,256]{2,1,0:T(8,128)(2,1)}, u32[]{:S(2)}) copy-start(bf16[1,2048,256]{2,1,0:T(8,128)(2,1)} %param.26) | copy-start | bytes 3145732
  7.2 88.2 %all-gather.5.cloned.1.call-start = ((), (), s32[]{:S(2)}) async-start(), calls=%async_computation.5 | async-start | bytes 4456448 | tf_op jit(solution)/shard_map/all_gather | solution.py:110
  99.9 1.3 copy-start.11
  107.0 4.9 %copy-start.2 = (bf16[512,128]{1,0:T(8,128)(2,1)S(1)}, bf16[512,128]{1,0:T(8,128)(2,1)}, u32[]{:S(2)}) copy-start(bf16[512,128]{1,0:T(8,128)(2,1)} %param.17) | copy-start | bytes 393220
  107.0 5.0 %copy-start.3 = (bf16[512,128]{1,0:T(8,128)(2,1)S(1)}, bf16[512,128]{1,0:T(8,128)(2,1)}, u32[]{:S(2)}) copy-start(bf16[512,128]{1,0:T(8,128)(2,1)} %param.16) | copy-start | bytes 393220
  107.0 8.2 %copy-start.7 = (f32[31,128]{1,0:T(8,128)S(1)}, f32[31,128]{1,0:T(8,128)}, u32[]{:S(2)}) copy-start(f32[31,128]{1,0:T(8,128)} %param.18) | copy-start | bytes 47620
  107.0 206.1 %copy-start.9 = (f32[128]{0:T(128)S(1)}, f32[128]{0:T(128)}, u32[]{:S(2)}) copy-start(f32[128]{0:T(128)} %param.20) | copy-start | bytes 1540
  107.0 206.1 %copy-start.10 = (f32[128]{0:T(128)S(1)}, f32[128]{0:T(128)}, u32[]{:S(2)}) copy-start(f32[128]{0:T(128)} %param.19) | copy-start | bytes 1540
  107.0 207.0 %all-to-all-start.1 = ((bf16[16,1024,256]{1,2,0:T(8,128)(2,1)}), bf16[16,1024,256]{1,2,0:T(8,128)(2,1)}, u32[]{:S(2)}, u32[]{:S(2)}) async-start(bf16[16,1024,256]{1,2,0:T(8,128)(2,1)} %stack.2), calls=%async_computation.1 | async-start | bytes 16777216 | tf_op jit(solution)/shard_map/all_to_all | solution.py:123
  111.9 247.8 %all-gather.3.cloned.1.call-start = ((), (), s32[]{:S(2)}) async-start(), calls=%async_computation.4 | async-start | bytes 2228224 | tf_op jit(solution)/shard_map/all_gather | solution.py:81
  112.1 3.9 %collective-permute-start = (bf16[30,128]{1,0:T(8,128)(2,1)S(1)}, bf16[30,128]{1,0:T(8,128)(2,1)S(1)}, u32[]{:S(2)}, u32[]{:S(2)}) collective-permute-start(bf16[30,128]{1,0:T(8,128)(2,1)S(1)} %slice.260), channel_id=1, source_target_pairs={{0,16},{16,32},{32,48},{48,64},{64,80},{80,96},{96,112},{112,128},... | collective-permute-start | bytes 23048 | tf_op jit(solution)/shard_map/ppermute | solution.py:13
  314.0 14.1 %copy-start.4 = (bf16[2048,32]{0,1:T(8,128)(2,1)S(1)}, bf16[2048,32]{0,1:T(8,128)(2,1)}, u32[]{:S(2)}) copy-start(bf16[2048,32]{0,1:T(8,128)(2,1)} %param.29) | copy-start | bytes 393220
  314.0 14.4 %copy-start.8 = (f32[128,4]{0,1:T(4,128)S(1)}, f32[128,4]{0,1:T(4,128)}, u32[]{:S(2)}) copy-start(f32[128,4]{0,1:T(4,128)} %param.25) | copy-start | bytes 6148
  314.0 14.5 %copy-start.5 = (bf16[2048,32]{0,1:T(8,128)(2,1)S(1)}, bf16[2048,32]{0,1:T(8,128)(2,1)}, u32[]{:S(2)}) copy-start(bf16[2048,32]{0,1:T(8,128)(2,1)} %param.30) | copy-start | bytes 393220
  314.1 45.7 %copy-start.1 = (bf16[2048,128]{1,0:T(8,128)(2,1)S(1)}, bf16[2048,128]{1,0:T(8,128)(2,1)}, u32[]{:S(2)}) copy-start(bf16[2048,128]{1,0:T(8,128)(2,1)} %param.21) | copy-start | bytes 1572868
  320.9 43.5 %copy-start.6 = (bf16[512,128]{1,0:T(8,128)(2,1)S(1)}, bf16[512,128]{1,0:T(8,128)(2,1)}, u32[]{:S(2)}) copy-start(bf16[512,128]{1,0:T(8,128)(2,1)} %param.31) | copy-start | bytes 393220
  320.9 24.4 %all-to-all-start.2 = ((bf16[8,4,1,32,128]{4,3,1,2,0:T(8,128)(2,1)}), bf16[8,4,1,32,128]{4,3,1,2,0:T(8,128)(2,1)S(1)}, u32[]{:S(2)}, u32[]{:S(2)}) async-start(bf16[8,4,1,32,128]{4,3,1,2,0:T(8,128)(2,1)} %bitcast.43), calls=%async_computation.2 | async-start | bytes 524288 | tf_op jit(solution)/shard_map/all_to_all | solution.py:31
  346.0 16.7 %all-to-all-start.3 = ((bf16[8,4,1,32,128]{4,3,0,2,1:T(8,128)(2,1)}), bf16[8,4,1,32,128]{4,3,0,2,1:T(8,128)(2,1)S(1)}, u32[]{:S(2)}, u32[]{:S(2)}) async-start(bf16[8,4,1,32,128]{4,3,0,2,1:T(8,128)(2,1)} %copy.42), calls=%async_computation.3 | async-start | bytes 524288 | tf_op jit(solution)/shard_map/all_to_all | solution.py:31
Sparse Core Ops, SparseCore 0:
  53.3 42.0 all-gather.4
  314.1 45.5 all-gather.2
